TPU v7x, 32 devices: a whole 2x2x4 slice. The times are simulated.
32 devices in a mesh: ep: 4 (over y, x), tp: 8 (over z, core).
Axes of the slice: x: 2, y: 2, z: 4, core: 2. Of those that a mesh axis runs over, the one named last changes fastest.
Arguments:
- queries: bfloat16 [4096, 1024], P('ep', 'tp'), may hold values from -6 to 6
- keys: bfloat16 [4096, 256], P('ep'), may hold values from -6 to 6, as said below
- values: bfloat16 [4096, 256], P('ep'), may hold values from -6 to 6
- slopes: float32 [16], P('tp'), may hold values from 0.002 to 0.08
- sinks: float32 [16], P('tp'), may hold values from 2 to 6
- out_weight: bfloat16 [1024, 2048], P('tp'), may hold values from -0.1875 to 0.1875
- mix_gain: float32 [2048], replicated, may hold values from 0.1 to 1.9
- moe_input: bfloat16 [4096, 2048], P(('ep', 'tp')), may hold values from -6 to 6
- in_gain: float32 [2048], replicated, may hold values from 0.1 to 1.9
- out_gain: float32 [2048], replicated, may hold values from 0.1 to 1.9
- group_router: bfloat16 [2048, 4], replicated, may hold values from -0.125 to 0.125
- expert_router: bfloat16 [2048, 4], replicated, may hold values from -0.125 to 0.125
- routes: int32 [4096, 2], P(('ep', 'tp')), may hold values from 0 to 3, all different within a row; in each aligned block of 128 rows (0 to 127, 128 to 255, ...) at most 96 rows name the same one
- gate_weight: bfloat16 [4, 2048, 1024], P('ep', None, 'tp'), may hold values from -0.125 to 0.125
- up_weight: bfloat16 [4, 2048, 1024], P('ep', None, 'tp'), may hold values from -0.125 to 0.125
- down_weight: bfloat16 [4, 2048, 1024], P('ep', None, 'tp'), may hold values from -0.1875 to 0.1875
Outputs:
- mixer_output: bfloat16 [4096, 2048], P(('ep', 'tp'))
- moe_output: bfloat16 [4096, 2048], P(('ep', 'tp'))
Inputs may be any that keep to these rules, and one draw needn't show every extreme that they name: `keys`: keys share one value range with the queries. `routes`: A token names 2 different experts. Among the rows of one device no expert is named more than 96 times, a bound that some block reaches in every draw.
All inputs are finite; a program needn't handle non-finite values.
Results may differ from a plain program's by a relative error of at most 0.018.
Values may be sent and summed in bfloat16 or wider, within the bound.
No kernel may reach another device: no remote copies, remote signals or barrier semaphores. Data moves between devices by JAX's collectives and lax.ppermute only.
A program may use at most 128 MiB of HBM per device.

v0:
```python
import math
import jax
import jax.numpy as jnp
from jax import lax
from jax.sharding import PartitionSpec as P

HEADS = 16
HD = 64
KV_HEADS = 4
WINDOW = 128
eps = 1e-06


def shifted(block, axis, distance):
    devices = range(lax.axis_size(axis))
    route = [(i - distance, i) for i in devices if i - distance in devices]
    return lax.ppermute(block, axis, route)


def scale_rows(matrix, gain):
    mean_square = jnp.mean(matrix * matrix, axis=-1, keepdims=True)
    return matrix * lax.rsqrt(mean_square + eps) * gain


def per_device(
    queries,
    keys,
    values,
    slopes,
    sinks,
    out_weight,
    mix_gain,
    moe_input,
    in_gain,
    out_gain,
    group_router,
    expert_router,
    routes,
    gate_weight,
    up_weight,
    down_weight,
):
    rows_group = queries.shape[0]
    local_heads = slopes.shape[0]
    per_kv = HEADS // KV_HEADS
    kv_index = lax.axis_index("tp") * local_heads // per_kv
    own_keys = lax.dynamic_slice_in_dim(keys, kv_index * HD, HD, 1)
    own_values = lax.dynamic_slice_in_dim(values, kv_index * HD, HD, 1)
    rim_keys, rim_values = shifted(
        (own_keys[rows_group - WINDOW :], own_values[rows_group - WINDOW :]), "ep", 1
    )
    blocks = rows_group // WINDOW
    key_blocks = own_keys.reshape(blocks, WINDOW, HD)
    value_blocks = own_values.reshape(blocks, WINDOW, HD)
    key_span = jnp.concatenate(
        [jnp.concatenate([rim_keys[None], key_blocks[:-1]], axis=0), key_blocks], axis=1
    )
    value_span = jnp.concatenate(
        [jnp.concatenate([rim_values[None], value_blocks[:-1]], axis=0), value_blocks], axis=1
    )
    query_blocks = queries.reshape(blocks, WINDOW, local_heads, HD)
    scores = jnp.einsum(
        "nqhd,nsd->nhqs", query_blocks, key_span, preferred_element_type=jnp.float32
    ) * (1.0 / math.sqrt(HD))
    query_index = jnp.arange(WINDOW, dtype=jnp.int32)[:, None]
    key_index = jnp.arange(2 * WINDOW, dtype=jnp.int32)[None, :]
    distance = query_index + WINDOW - key_index
    key_position = (
        lax.axis_index("ep") * rows_group
        + jnp.arange(blocks, dtype=jnp.int32)[:, None, None] * WINDOW
        + key_index[None]
        - WINDOW
    )
    valid = ((distance >= 0) & (distance < WINDOW))[None] & (key_position >= 0)
    scores = scores - slopes[None, :, None, None] * distance.astype(jnp.float32)[None, None]
    scores = jnp.where(valid[:, None], scores, -jnp.inf)
    sink = sinks[None, :, None, None]
    top = jnp.maximum(jnp.max(scores, axis=-1, keepdims=True), sink)
    weights = jnp.exp(scores - top)
    denom = jnp.sum(weights, axis=-1, keepdims=True) + jnp.exp(sink - top)
    probs = (weights / denom).astype(jnp.bfloat16)
    attention = jnp.einsum("nhqs,nsd->nqhd", probs, value_span, preferred_element_type=jnp.float32)
    attention = attention.astype(jnp.bfloat16).reshape(rows_group, local_heads * HD)
    own_rows = moe_input.shape[0]
    projected = lax.psum_scatter(
        jnp.dot(attention, out_weight, preferred_element_type=jnp.float32).astype(jnp.bfloat16),
        "tp",
        scatter_dimension=0,
        tiled=True,
    ).astype(jnp.float32)
    mixer_output = scale_rows(projected, mix_gain).astype(jnp.bfloat16)
    normed = scale_rows(moe_input.astype(jnp.float32), in_gain).astype(jnp.bfloat16)
    group_logits = jnp.dot(normed, group_router, preferred_element_type=jnp.float32)
    expert_logits = jnp.dot(normed, expert_router, preferred_element_type=jnp.float32)
    experts = expert_router.shape[1]
    groups = group_router.shape[1]
    per_group = experts // groups
    visits = routes.shape[1]
    expert_match = routes[:, :, None] == jnp.arange(experts, dtype=jnp.int32)[None, None, :]
    picked_logits = jnp.sum(jnp.where(expert_match, expert_logits[:, None, :], 0.0), axis=-1)
    group_prob = jax.nn.softmax(group_logits, axis=-1)
    group_match = (routes // per_group)[:, :, None] == jnp.arange(groups, dtype=jnp.int32)[
        None, None, :
    ]
    picked_group = jnp.sum(jnp.where(group_match, group_prob[:, None, :], 0.0), axis=-1)
    route_weight = picked_group * jax.nn.softmax(picked_logits, axis=-1)
    capacity = max(2, 3 * own_rows * visits // (2 * experts))
    match_int = expert_match.astype(jnp.int32).reshape(own_rows * visits, experts)
    before = jnp.cumsum(match_int, axis=0) - match_int
    slot = jnp.sum(before * match_int, axis=-1)
    position = (routes.reshape(-1) * capacity + slot).reshape(own_rows, visits)
    slot_ids = jnp.arange(experts * capacity, dtype=jnp.int32)
    placement = jnp.any(position[None, :, :] == slot_ids[:, None, None], axis=-1).astype(
        jnp.bfloat16
    )
    outgoing = jnp.dot(placement, normed, preferred_element_type=jnp.float32).astype(jnp.bfloat16)
    local_experts = gate_weight.shape[0]
    outgoing = outgoing.reshape(lax.axis_size("ep"), local_experts, capacity, normed.shape[1])
    arrived = lax.all_to_all(outgoing, "ep", split_axis=0, concat_axis=0, tiled=True)
    gate_piece = lax.all_gather(gate_weight, "tp", axis=2, tiled=True)
    up_piece = lax.all_gather(up_weight, "tp", axis=2, tiled=True)
    down_piece = lax.all_gather(down_weight, "tp", axis=2, tiled=True)
    gate = jnp.einsum("sxcd,xdf->sxcf", arrived, gate_piece, preferred_element_type=jnp.float32)
    up = jnp.einsum("sxcd,xdf->sxcf", arrived, up_piece, preferred_element_type=jnp.float32)
    hidden = (jax.nn.silu(gate) * up).astype(jnp.bfloat16)
    results = jnp.einsum("sxcf,xdf->sxcd", hidden, down_piece, preferred_element_type=jnp.float32)
    returned = lax.all_to_all(
        results.astype(jnp.bfloat16), "ep", split_axis=0, concat_axis=0, tiled=True
    )
    flat_back = returned.reshape(experts * capacity, returned.shape[3])
    picked_rows = jnp.take(flat_back, position.reshape(-1), axis=0).reshape(
        own_rows, visits, flat_back.shape[1]
    )
    moe = jnp.sum(route_weight[:, :, None] * picked_rows.astype(jnp.float32), axis=1)
    moe_output = scale_rows(moe, out_gain).astype(jnp.bfloat16)
    return (mixer_output, moe_output)


def solution(mesh):
    return jax.shard_map(
        per_device,
        mesh=mesh,
        in_specs=(
            P("ep", "tp"),
            P("ep", None),
            P("ep", None),
            P("tp"),
            P("tp"),
            P("tp", None),
            P(),
            P(("ep", "tp"), None),
            P(),
            P(),
            P(),
            P(),
            P(("ep", "tp"), None),
            P("ep", None, "tp"),
            P("ep", None, "tp"),
            P("ep", None, "tp"),
        ),
        out_specs=(P(("ep", "tp"), None), P(("ep", "tp"), None)),
        check_vma=False,
    )
```

profile of v0, /device:TPU:0, one launch (start us, length us, event | category | flops | bytes accessed | tf_op | source)
XLA Modules:
  0.0 222.8 jit_solution(3067624268574023449)
XLA Ops:
  7.2 0.7 all-gather.6.cloned.1.call-update
  8.0 0.7 all-gather.4.cloned.1.call-update
  8.7 0.7 all-gather.8.cloned.1.call-update
  9.5 1.2 constant_dynamic-slice_fusion
  10.9 4.9 %collective-permute-start.1 = (bf16[128,64]{0,1:T(8,128)(2,1)S(1)}, bf16[128,64]{0,1:T(8,128)(2,1)S(1)}, u32[]{:S(2)}, u32[]{:S(2)}) collective-permute-start(bf16[128,64]{0,1:T(8,128)(2,1)S(1)} %slice.36), channel_id=1, source_target_pairs={{0,8},{8,16},{16,24},{1,9},{9,17},{17,25},{2,10},{10,18},{18,26},{... | collective-permute-start | bytes 49160 | tf_op jit(solution)/shard_map/ppermute | solution.py:17
  15.9 3.4 %collective-permute-start = (bf16[128,64]{0,1:T(8,128)(2,1)S(1)}, bf16[128,64]{0,1:T(8,128)(2,1)S(1)}, u32[]{:S(2)}, u32[]{:S(2)}) collective-permute-start(bf16[128,64]{0,1:T(8,128)(2,1)S(1)} %slice.34), channel_id=1, source_target_pairs={{0,8},{8,16},{16,24},{1,9},{9,17},{17,25},{2,10},{10,18},{18,26},{... | collective-permute-start | bytes 49160 | tf_op jit(solution)/shard_map/ppermute | solution.py:17
  22.2 3.2 %convolution_convert_fusion = bf16[1024,2048]{1,0:T(8,128)(2,1)} fusion(bf16[128,2048]{1,0:T(8,128)(2,1)S(1)} %copy-done, bf16[16,8,8,128]{3,2,1,0:T(8,128)(2,1)S(1)} %bitcast.155), kind=kOutput, calls=%fused_computation.7 | convolution fusion | flops 538968064 | bytes 4980736 | tf_op jit(solution)/shard_map/dot_general | solution.py:86
  26.5 1.2 reduce-window.6
  28.6 1.8 convolution_convert_fusion.1
  30.4 3.9 %all-to-all-start = ((bf16[4,1,96,2048]{3,2,1,0:T(8,128)(2,1)}), bf16[4,1,96,2048]{3,2,1,0:T(8,128)(2,1)S(1)}, u32[]{:S(2)}, u32[]{:S(2)}) async-start(bf16[4,1,96,2048]{3,2,1,0:T(8,128)(2,1)} %bitcast.11), calls=%async_computation.1 | async-start | bytes 3145728 | tf_op jit(solution)/shard_map/all_to_all | solution.py:119
  35.5 17.6 %all-to-all-done = bf16[4,1,96,2048]{3,2,1,0:T(8,128)(2,1)S(1)} async-done(((bf16[4,1,96,2048]{3,2,1,0:T(8,128)(2,1)}), bf16[4,1,96,2048]{3,2,1,0:T(8,128)(2,1)S(1)}, u32[]{:S(2)}, u32[]{:S(2)}) %all-to-all-start) | async-done | bytes 1572896 | tf_op jit(solution)/shard_map/all_to_all | solution.py:119
  53.1 7.1 %all-gather.6.cloned.1.call-done = bf16[1,2048,1024]{2,1,0:T(8,128)(2,1)} async-done(((bf16[1,2048,128]{2,1,0:T(8,128)(2,1)}), bf16[1,2048,1024]{2,1,0:T(8,128)(2,1)}) %all-gather.6.cloned.1.call-update) | async-done | bytes 4194320 | tf_op jit(solution)/shard_map/all_gather | solution.py:121
  60.2 5.1 %fusion.2 = f32[4,96,1024]{2,1,0:T(8,128)} fusion(bf16[1,2048,1024]{2,1,0:T(8,128)(2,1)} %all-gather.6.cloned.1.call-done, bf16[4,1,96,2048]{3,2,1,0:T(8,128)(2,1)S(1)} %all-to-all-done), kind=kOutput, calls=%fused_computation.3 | convolution fusion | flops 1610612736 | bytes 7340032 | tf_op jit(solution)/shard_map/sxcd,xdf->sxcf/dot_general | solution.py:124
  65.3 42.5 %all-gather.4.cloned.1.call-done = bf16[1,2048,1024]{2,1,0:T(8,128)(2,1)} async-done(((bf16[1,2048,128]{2,1,0:T(8,128)(2,1)}), bf16[1,2048,1024]{2,1,0:T(8,128)(2,1)}) %all-gather.4.cloned.1.call-update) | async-done | bytes 4194320 | tf_op jit(solution)/shard_map/all_gather | solution.py:120
  107.8 47.6 %all-gather.8.cloned.1.call-done = bf16[1,2048,1024]{2,1,0:T(8,128)(2,1)} async-done(((bf16[1,2048,128]{2,1,0:T(8,128)(2,1)}), bf16[1,2048,1024]{2,1,0:T(8,128)(2,1)}) %all-gather.8.cloned.1.call-update) | async-done | bytes 4194320 | tf_op jit(solution)/shard_map/all_gather | solution.py:122
  155.4 8.6 %fusion.9 = bf16[4,1,96,2048]{3,2,1,0:T(8,128)(2,1)} fusion(bf16[1,2048,1024]{2,1,0:T(8,128)(2,1)} %all-gather.8.cloned.1.call-done, f32[4,96,1024]{2,1,0:T(8,128)} %fusion.2, bf16[1,2048,1024]{2,1,0:T(8,128)(2,1)} %all-gather.4.cloned.1.call-done, bf16[4,1,96,2048]{3,2,1,0:T(8,128)(2,1)S(1)} %all-to-all-done), kind=kOutput, calls=%fused_computation.10 | convolution fusion | flops 3224371200 | bytes 13107200 | tf_op jit(solution)/shard_map/sxcf,xdf->sxcd/dot_general | solution.py:126
  164.1 3.9 %all-to-all-start.1 = ((bf16[4,1,96,2048]{3,2,1,0:T(8,128)(2,1)}), bf16[4,1,96,2048]{3,2,1,0:T(8,128)(2,1)S(1)}, u32[]{:S(2)}, u32[]{:S(2)}) async-start(bf16[4,1,96,2048]{3,2,1,0:T(8,128)(2,1)} %fusion.9), calls=%async_computation.2 | async-start | bytes 3145728 | tf_op jit(solution)/shard_map/all_to_all | solution.py:127
  168.1 37.6 %reduce-scatter.2.cloned.1.call-done = bf16[128,2048]{1,0:T(8,128)(2,1)} async-done(((bf16[1024,2048]{1,0:T(8,128)(2,1)}), bf16[128,2048]{1,0:T(8,128)(2,1)}) %reduce-scatter.2.cloned.1.call-update) | async-done | bytes 524304 | tf_op jit(solution)/shard_map/reduce_scatter | solution.py:85
  205.7 1.2 fusion.30
  207.0 2.0 fusion.32
  209.0 1.4 gather_fusion
  210.4 0.7 gather.7
  211.1 4.1 %multiply_reduce_fusion = f32[128,2048]{1,0:T(8,128)S(1)} fusion(bf16[128,2,2048]{2,1,0:T(2,128)(2,1)S(1)} %gather.7, pred[128,2]{1,0:T(8,128)(4,1)S(1)} %copy.102, f32[128,2]{1,0:T(8,128)S(1)} %copy.96), kind=kLoop, calls=%fused_computation.13 | loop fusion | flops 1835008 | bytes 2098432 | tf_op jit(solution)/shard_map/reduce_sum | solution.py:134
  215.3 1.0 multiply_convert_fusion
  (87 shorter events, 6.6 us)
Async XLA Ops:
  7.2 15.0 %copy-start = (bf16[128,2048]{1,0:T(8,128)(2,1)S(1)}, bf16[128,2048]{1,0:T(8,128)(2,1)}, u32[]{:S(2)}) copy-start(bf16[128,2048]{1,0:T(8,128)(2,1)} %param.21) | copy-start | bytes 1572868
  7.2 53.0 %all-gather.6.cloned.1.call-start = ((), (), s32[]{:S(2)}) async-start(), calls=%async_computation.5 | async-start | bytes 4718592 | tf_op jit(solution)/shard_map/all_gather | solution.py:121
  7.9 12.0 %copy-start.8 = (f32[2]{0:T(128)S(1)}, f32[2]{0:T(128)}, u32[]{:S(2)}) copy-start(f32[2]{0:T(128)} %param.19) | copy-start | bytes 28
  7.9 99.9 %all-gather.4.cloned.1.call-start = ((), (), s32[]{:S(2)}) async-start(), calls=%async_computation.4 | async-start | bytes 4718592 | tf_op jit(solution)/shard_map/all_gather | solution.py:120
  8.7 11.4 %copy-start.2 = (bf16[1024,128]{1,0:T(8,128)(2,1)S(1)}, bf16[1024,128]{1,0:T(8,128)(2,1)}, u32[]{:S(2)}) copy-start(bf16[1024,128]{1,0:T(8,128)(2,1)} %param.16) | copy-start | bytes 786436
  8.7 146.7 %all-gather.8.cloned.1.call-start = ((), (), s32[]{:S(2)}) async-start(), calls=%async_computation.6 | async-start | bytes 4718592 | tf_op jit(solution)/shard_map/all_gather | solution.py:122
  9.4 196.3 %reduce-scatter.2.cloned.1.call-start = ((), (), s32[]{:S(2)}) async-start(), calls=%async_computation.3 | async-start | bytes 4718592 | tf_op jit(solution)/shard_map/reduce_scatter | solution.py:85
  10.9 9.4 %collective-permute-start.1 = (bf16[128,64]{0,1:T(8,128)(2,1)S(1)}, bf16[128,64]{0,1:T(8,128)(2,1)S(1)}, u32[]{:S(2)}, u32[]{:S(2)}) collective-permute-start(bf16[128,64]{0,1:T(8,128)(2,1)S(1)} %slice.36), channel_id=1, source_target_pairs={{0,8},{8,16},{16,24},{1,9},{9,17},{17,25},{2,10},{10,18},{18,26},{... | collective-permute-start | bytes 49160 | tf_op jit(solution)/shard_map/ppermute | solution.py:17
  15.9 5.6 %collective-permute-start = (bf16[128,64]{0,1:T(8,128)(2,1)S(1)}, bf16[128,64]{0,1:T(8,128)(2,1)S(1)}, u32[]{:S(2)}, u32[]{:S(2)}) collective-permute-start(bf16[128,64]{0,1:T(8,128)(2,1)S(1)} %slice.34), channel_id=1, source_target_pairs={{0,8},{8,16},{16,24},{1,9},{9,17},{17,25},{2,10},{10,18},{18,26},{... | collective-permute-start | bytes 49160 | tf_op jit(solution)/shard_map/ppermute | solution.py:17
  20.3 0.7 copy-start.7
  25.4 0.7 copy-start.3
  25.4 3.0 %copy-start.1 = (bf16[128,2048]{1,0:T(8,128)(2,1)S(1)}, bf16[128,2048]{1,0:T(8,128)(2,1)}, u32[]{:S(2)}) copy-start(bf16[128,2048]{1,0:T(8,128)(2,1)} %param.23) | copy-start | bytes 1572868
  25.4 3.2 %copy-start.4 = (f32[2048]{0:T(1024)S(1)}, f32[2048]{0:T(1024)}, u32[]{:S(2)}) copy-start(f32[2048]{0:T(1024)} %param.24) | copy-start | bytes 24580
  30.4 3.9 %copy-start.9 = (bf16[2048,4]{0,1:T(4,128)(2,1)S(1)}, bf16[2048,4]{0,1:T(4,128)(2,1)}, u32[]{:S(2)}) copy-start(bf16[2048,4]{0,1:T(4,128)(2,1)} %param.26) | copy-start | bytes 49156
  30.4 4.3 %copy-start.10 = (bf16[2048,4]{0,1:T(4,128)(2,1)S(1)}, bf16[2048,4]{0,1:T(4,128)(2,1)}, u32[]{:S(2)}) copy-start(bf16[2048,4]{0,1:T(4,128)(2,1)} %param.27) | copy-start | bytes 49156
  30.4 22.6 %all-to-all-start = ((bf16[4,1,96,2048]{3,2,1,0:T(8,128)(2,1)}), bf16[4,1,96,2048]{3,2,1,0:T(8,128)(2,1)S(1)}, u32[]{:S(2)}, u32[]{:S(2)}) async-start(bf16[4,1,96,2048]{3,2,1,0:T(8,128)(2,1)} %bitcast.11), calls=%async_computation.1 | async-start | bytes 3145728 | tf_op jit(solution)/shard_map/all_to_all | solution.py:119
  164.1 42.9 %copy-start.5 = (f32[2048]{0:T(1024)S(1)}, f32[2048]{0:T(1024)}, u32[]{:S(2)}) copy-start(f32[2048]{0:T(1024)} %param.22) | copy-start | bytes 24580
  164.1 44.9 %all-to-all-start.1 = ((bf16[4,1,96,2048]{3,2,1,0:T(8,128)(2,1)}), bf16[4,1,96,2048]{3,2,1,0:T(8,128)(2,1)S(1)}, u32[]{:S(2)}, u32[]{:S(2)}) async-start(bf16[4,1,96,2048]{3,2,1,0:T(8,128)(2,1)} %fusion.9), calls=%async_computation.2 | async-start | bytes 3145728 | tf_op jit(solution)/shard_map/all_to_all | solution.py:127
  211.1 4.3 %copy-start.6 = (f32[2048]{0:T(1024)S(1)}, f32[2048]{0:T(1024)}, u32[]{:S(2)}) copy-start(f32[2048]{0:T(1024)} %param.25) | copy-start | bytes 24580
Sparse Core Ops, SparseCore 0:
  9.6 50.5 all-gather.5
  61.7 45.9 all-gather.3
  109.4 45.9 all-gather.7
  157.6 48.1 reduce-scatter.1
where the time goes:
time: 223 us
  waiting for transfers between devices  155 us (70%)
  matrix products  20.5 us (9%)
  starting transfers between devices  16.2 us (7%)
  between operations  14.2 us (6%)
  other arithmetic  11.3 us (5%)
  local copies, waits for them, and re-layouts  6.18 us (3%)
    all_gather x1, waiting for transfers between devices, per_device(): down_piece = lax.all_gather(down_weight, 'tp', axis=2, tiled=True)  47.6 us
    all_gather x1, waiting for transfers between devices, per_device(): gate_piece = lax.all_gather(gate_weight, 'tp', axis=2, tiled=True)  42.5 us
    reduce_scatter x1, waiting for transfers between devices, per_device(): lax.psum_scatter(jnp.dot(attention, out_weight, preferred_element_type=jn...  37.6 us
    all_to_all x1, waiting for transfers between devices, per_device(): lax.all_to_all(outgoing, 'ep', split_axis=0, concat_axis=0, tiled=True)  17.6 us
    dot_general x1, matrix products, per_device(): jnp.einsum('sxcf,xdf->sxcd', hidden, down_piece, preferred_element_type=j...  8.63 us
    ppermute x2, starting transfers between devices, shifted(): return lax.ppermute(block, axis, route)  8.27 us
    all_gather x1, waiting for transfers between devices, per_device(): up_piece = lax.all_gather(up_weight, 'tp', axis=2, tiled=True)  7.09 us
    dot_general x1, matrix products, per_device(): jnp.einsum('sxcd,xdf->sxcf', arrived, up_piece, preferred_element_type=jn...  5.13 us
  transfers between devices with their start and end apart: 8, of which 5 were waited for; matrix products, arithmetic and copies ran while one was open for 13% of the time, Pallas kernels for 0%

commit v1 on v0

--- a/solution.py
+++ b/solution.py
@@ -117,7 +117,16 @@
     local_experts = gate_weight.shape[0]
     outgoing = outgoing.reshape(lax.axis_size("ep"), local_experts, capacity, normed.shape[1])
     arrived = lax.all_to_all(outgoing, "ep", split_axis=0, concat_axis=0, tiled=True)
-    gate_piece = lax.all_gather(gate_weight, "tp", axis=2, tiled=True)
+    array = gate_weight
+    ways, here, step = (lax.axis_size("tp"), lax.axis_index("tp"), array.shape[2])
+    lengths = [n * ways if d == 2 else n for d, n in enumerate(array.shape)]
+    full = lax.dynamic_update_slice_in_dim(
+        jnp.zeros(lengths, array.dtype), array, here * step, axis=2
+    )
+    for far in range(1, ways):
+        array = lax.ppermute(array, "tp", [(d, (d + 1) % ways) for d in range(ways)])
+        full = lax.dynamic_update_slice_in_dim(full, array, (here - far) % ways * step, axis=2)
+    gate_piece = full
     up_piece = lax.all_gather(up_weight, "tp", axis=2, tiled=True)
     down_piece = lax.all_gather(down_weight, "tp", axis=2, tiled=True)
     gate = jnp.einsum("sxcd,xdf->sxcf", arrived, gate_piece, preferred_element_type=jnp.float32)

time: 223 us -> 195 us (0.87)
  waiting for transfers between devices: 155 us -> 113 us
  local copies, waits for them, and re-layouts: 6.18 us -> 17.9 us
    ppermute x0 -> x7, waiting for transfers between devices: none -> 88 us  [per_device(): lax.ppermute(array, 'tp', [(d, (d + 1) % ways) for d in range(ways)])]
    all_gather x1, waiting for transfers between devices: 47.6 us -> 0.01 us  [per_device(): down_piece = lax.all_gather(down_weight, 'tp', axis=2, tiled=True)]
    all_gather x1 -> x0, waiting for transfers between devices: 42.5 us -> none  [per_device(): gate_piece = lax.all_gather(gate_weight, 'tp', axis=2, tiled=True)]
    all_to_all x1, waiting for transfers between devices: 17.6 us -> 0.01 us  [per_device(): lax.all_to_all(outgoing, 'ep', split_axis=0, concat_axis=0, tiled=True)]
    reduce_scatter x1, waiting for transfers between devices: 37.6 us -> 23.7 us  [per_device(): lax.psum_scatter(jnp.dot(attention, out_weight, preferred_element_type=jn...]
    dynamic_update_slice x0 -> x8, local copies, waits for them, and re-layouts: none -> 9.19 us  [the longest x7 8.25 us: per_device(): lax.dynamic_update_slice_in_dim(full, array, (here - far) % ways * step,...]
    all_gather x1, waiting for transfers between devices: 7.09 us -> 0.01 us  [per_device(): up_piece = lax.all_gather(up_weight, 'tp', axis=2, tiled=True)]
    another operation x2 -> x3, local copies, waits for them, and re-layouts: 0.1 us -> 2.59 us
  transfers between devices with their start and end apart: 8 -> 14, of which waited for: 5 -> 7; matrix products, arithmetic and copies ran while one was open for 13% -> 22% of each run, Pallas kernels for 0% -> 0%
where the time goes in v1:
time: 195 us
  waiting for transfers between devices  113 us (58%)
  matrix products  20.8 us (11%)
  local copies, waits for them, and re-layouts  17.9 us (9%)
  starting transfers between devices  17.3 us (9%)
  between operations  14.2 us (7%)
  other arithmetic  11.2 us (6%)
    ppermute x7, waiting for transfers between devices, per_device(): lax.ppermute(array, 'tp', [(d, (d + 1) % ways) for d in range(ways)])  88 us
    reduce_scatter x1, waiting for transfers between devices, per_device(): lax.psum_scatter(jnp.dot(attention, out_weight, preferred_element_type=jn...  23.7 us
    dot_general x1, matrix products, per_device(): jnp.einsum('sxcf,xdf->sxcd', hidden, down_piece, preferred_element_type=j...  8.86 us
    dynamic_update_slice x7, local copies, waits for them, and re-layouts, per_device(): lax.dynamic_update_slice_in_dim(full, array, (here - far) % ways * step,...  8.25 us
    ppermute x2, starting transfers between devices, shifted(): return lax.ppermute(block, axis, route)  7.82 us
    dot_general x1, matrix products, per_device(): jnp.einsum('sxcd,xdf->sxcf', arrived, up_piece, preferred_element_type=jn...  5.13 us
    reduce_sum x1, other arithmetic, per_device(): jnp.sum(route_weight[:, :, None] * picked_rows.astype(jnp.float32), axis=1)  4.07 us
    all_to_all x1, starting transfers between devices, per_device(): lax.all_to_all(results.astype(jnp.bfloat16), 'ep', split_axis=0, concat_a...  4 us
  transfers between devices with their start and end apart: 14, of which 7 were waited for; matrix products, arithmetic and copies ran while one was open for 22% of the time, Pallas kernels for 0%

profile of v1, /device:TPU:0, one launch (start us, length us, event | category | flops | bytes accessed | tf_op | source)
XLA Modules:
  0.0 194.6 jit_solution(6662852009122302607)
XLA Ops:
  9.3 1.2 constant_dynamic-slice_fusion
  10.7 4.4 %collective-permute-start.1 = (bf16[128,64]{0,1:T(8,128)(2,1)S(1)}, bf16[128,64]{0,1:T(8,128)(2,1)S(1)}, u32[]{:S(2)}, u32[]{:S(2)}) collective-permute-start(bf16[128,64]{0,1:T(8,128)(2,1)S(1)} %slice.36), channel_id=1, source_target_pairs={{0,8},{8,16},{16,24},{1,9},{9,17},{17,25},{2,10},{10,18},{18,26},{... | collective-permute-start | bytes 49160 | tf_op jit(solution)/shard_map/ppermute | solution.py:17
  15.3 3.4 %collective-permute-start = (bf16[128,64]{0,1:T(8,128)(2,1)S(1)}, bf16[128,64]{0,1:T(8,128)(2,1)S(1)}, u32[]{:S(2)}, u32[]{:S(2)}) collective-permute-start(bf16[128,64]{0,1:T(8,128)(2,1)S(1)} %slice.34), channel_id=1, source_target_pairs={{0,8},{8,16},{16,24},{1,9},{9,17},{17,25},{2,10},{10,18},{18,26},{... | collective-permute-start | bytes 49160 | tf_op jit(solution)/shard_map/ppermute | solution.py:17
  19.8 1.2 reduce-window.6
  23.5 3.2 %convolution_convert_fusion = bf16[1024,2048]{1,0:T(8,128)(2,1)} fusion(bf16[128,2048]{1,0:T(8,128)(2,1)S(1)} %copy-done, bf16[16,8,8,128]{3,2,1,0:T(8,128)(2,1)S(1)} %bitcast.168), kind=kOutput, calls=%fused_computation.7 | convolution fusion | flops 538968064 | bytes 4980736 | tf_op jit(solution)/shard_map/dot_general | solution.py:86
  28.0 1.8 convolution_convert_fusion.1
  29.8 3.7 %all-to-all-start = ((bf16[4,1,96,2048]{3,2,1,0:T(8,128)(2,1)}), bf16[4,1,96,2048]{3,2,1,0:T(8,128)(2,1)S(1)}, u32[]{:S(2)}, u32[]{:S(2)}) async-start(bf16[4,1,96,2048]{3,2,1,0:T(8,128)(2,1)} %bitcast.20), calls=%async_computation.1 | async-start | bytes 3145728 | tf_op jit(solution)/shard_map/all_to_all | solution.py:119
  35.3 20.0 %collective-permute-done.3 = bf16[1,2048,128]{2,1,0:T(8,128)(2,1)} collective-permute-done((bf16[1,2048,128]{2,1,0:T(8,128)(2,1)S(1)}, bf16[1,2048,128]{2,1,0:T(8,128)(2,1)}, u32[]{:S(2)}, u32[]{:S(2)}) %collective-permute-start.3) | collective-permute-done | bytes 524320 | tf_op jit(solution)/shard_map/ppermute | solution.py:127
  55.4 14.2 %collective-permute-done.4 = bf16[1,2048,128]{2,1,0:T(8,128)(2,1)S(1)} collective-permute-done((bf16[1,2048,128]{2,1,0:T(8,128)(2,1)}, bf16[1,2048,128]{2,1,0:T(8,128)(2,1)S(1)}, u32[]{:S(2)}, u32[]{:S(2)}) %collective-permute-start.4) | collective-permute-done | bytes 524320 | tf_op jit(solution)/shard_map/ppermute | solution.py:127
  70.0 2.5 %broadcast.267 = bf16[2048,1024]{1,0:T(8,128)(2,1)} broadcast(bf16[]{:T(256)} %constant.144.clone.1), dimensions={} | broadcast | bytes 4194306 | tf_op jit(solution)/shard_map/broadcast.120
  73.5 7.9 %collective-permute-done.5 = bf16[1,2048,128]{2,1,0:T(8,128)(2,1)} collective-permute-done((bf16[1,2048,128]{2,1,0:T(8,128)(2,1)S(1)}, bf16[1,2048,128]{2,1,0:T(8,128)(2,1)}, u32[]{:S(2)}, u32[]{:S(2)}) %collective-permute-start.5) | collective-permute-done | bytes 524320 | tf_op jit(solution)/shard_map/ppermute | solution.py:127
  82.2 1.9 bitcast_dynamic-update-slice_fusion.5
  84.1 18.4 %collective-permute-done.6 = bf16[1,2048,128]{2,1,0:T(8,128)(2,1)S(1)} collective-permute-done((bf16[1,2048,128]{2,1,0:T(8,128)(2,1)}, bf16[1,2048,128]{2,1,0:T(8,128)(2,1)S(1)}, u32[]{:S(2)}, u32[]{:S(2)}) %collective-permute-start.6) | collective-permute-done | bytes 524320 | tf_op jit(solution)/shard_map/ppermute | solution.py:127
  103.4 1.9 bitcast_dynamic-update-slice_fusion.3
  105.3 19.0 %collective-permute-done.7 = bf16[1,2048,128]{2,1,0:T(8,128)(2,1)S(1)} collective-permute-done((bf16[1,2048,128]{2,1,0:T(8,128)(2,1)S(1)}, bf16[1,2048,128]{2,1,0:T(8,128)(2,1)S(1)}, u32[]{:S(2)}, u32[]{:S(2)}) %collective-permute-start.7) | collective-permute-done | bytes 524320 | tf_op jit(solution)/shard_map/ppermute | solution.py:127
  126.0 8.7 %collective-permute-done.8 = bf16[1,2048,128]{2,1,0:T(8,128)(2,1)S(1)} collective-permute-done((bf16[1,2048,128]{2,1,0:T(8,128)(2,1)S(1)}, bf16[1,2048,128]{2,1,0:T(8,128)(2,1)S(1)}, u32[]{:S(2)}, u32[]{:S(2)}) %collective-permute-start.8) | collective-permute-done | bytes 524320 | tf_op jit(solution)/shard_map/ppermute | solution.py:127
  135.6 5.1 %fusion.2 = f32[4,96,1024]{2,1,0:T(8,128)} fusion(bf16[1,2048,1024]{2,1,0:T(8,128)(2,1)} %all-gather.3.cloned.1.call-done, bf16[4,1,96,2048]{3,2,1,0:T(8,128)(2,1)S(1)} %all-to-all-done), kind=kOutput, calls=%fused_computation.3 | convolution fusion | flops 1610612736 | bytes 7340032 | tf_op jit(solution)/shard_map/sxcd,xdf->sxcf/dot_general | solution.py:133
  140.7 8.9 %fusion.9 = bf16[4,1,96,2048]{3,2,1,0:T(8,128)(2,1)} fusion(bf16[1,2048,1024]{2,1,0:T(8,128)(2,1)} %all-gather.5.cloned.1.call-done, f32[4,96,1024]{2,1,0:T(8,128)} %fusion.2, bf16[4,1,96,2048]{3,2,1,0:T(8,128)(2,1)S(1)} %all-to-all-done, bf16[2048,1024]{1,0:T(8,128)(2,1)} %bitcast_dynamic-update-slice_fusion), kind=kOutput, calls=%fused_computation.10 | convolution fusion | flops 3224371200 | bytes 13107200 | tf_op jit(solution)/shard_map/sxcf,xdf->sxcd/dot_general | solution.py:135
  149.6 4.0 %all-to-all-start.1 = ((bf16[4,1,96,2048]{3,2,1,0:T(8,128)(2,1)}), bf16[4,1,96,2048]{3,2,1,0:T(8,128)(2,1)S(1)}, u32[]{:S(2)}, u32[]{:S(2)}) async-start(bf16[4,1,96,2048]{3,2,1,0:T(8,128)(2,1)} %fusion.9), calls=%async_computation.2 | async-start | bytes 3145728 | tf_op jit(solution)/shard_map/all_to_all | solution.py:136
  153.8 23.7 %reduce-scatter.2.cloned.1.call-done = bf16[128,2048]{1,0:T(8,128)(2,1)} async-done(((bf16[1024,2048]{1,0:T(8,128)(2,1)}), bf16[128,2048]{1,0:T(8,128)(2,1)}) %reduce-scatter.2.cloned.1.call-update) | async-done | bytes 524304 | tf_op jit(solution)/shard_map/reduce_scatter | solution.py:85
  177.5 1.2 fusion.21
  178.7 2.0 %fusion.23 = bf16[128,2048]{1,0:T(8,128)(2,1)} fusion(bf16[128,2048]{1,0:T(8,128)(2,1)} %reduce-scatter.2.cloned.1.call-done, f32[2048]{0:T(1024)S(1)} %copy-done.6, f32[128]{0:T(128)S(1)} %add_rsqrt_fusion.2), kind=kLoop, calls=%fused_computation.35 | loop fusion | flops 1048576 | bytes 1057280 | tf_op jit(solution)/shard_map/convert_element_type | solution.py:91
  180.7 1.4 gather_fusion
  182.8 4.1 %multiply_reduce_fusion = f32[128,2048]{1,0:T(8,128)S(1)} fusion(bf16[128,2,2048]{2,1,0:T(2,128)(2,1)S(1)} %gather.7, pred[128,2]{1,0:T(8,128)(4,1)S(1)} %copy.102, f32[128,2]{1,0:T(8,128)S(1)} %copy.96), kind=kLoop, calls=%fused_computation.13 | loop fusion | flops 1835008 | bytes 2098432 | tf_op jit(solution)/shard_map/reduce_sum | solution.py:143
  (109 shorter events, 16.7 us)
Async XLA Ops:
  7.2 16.3 %copy-start = (bf16[128,2048]{1,0:T(8,128)(2,1)S(1)}, bf16[128,2048]{1,0:T(8,128)(2,1)}, u32[]{:S(2)}) copy-start(bf16[128,2048]{1,0:T(8,128)(2,1)} %param.21) | copy-start | bytes 1572868
  7.2 11.5 %copy-start.4 = (s32[128,2]{0,1:T(2,128)S(1)}, s32[128,2]{0,1:T(2,128)}, u32[]{:S(2)}) copy-start(s32[128,2]{0,1:T(2,128)} %param.28) | copy-start | bytes 3076
  7.2 128.4 %all-gather.3.cloned.1.call-start = ((), (), s32[]{:S(2)}) async-start(), calls=%async_computation.4 | async-start | bytes 4718592 | tf_op jit(solution)/shard_map/all_gather | solution.py:130
  7.9 11.6 %copy-start.9 = (f32[2]{0:T(128)S(1)}, f32[2]{0:T(128)}, u32[]{:S(2)}) copy-start(f32[2]{0:T(128)} %param.19) | copy-start | bytes 28
  7.9 132.8 %all-gather.5.cloned.1.call-start = ((), (), s32[]{:S(2)}) async-start(), calls=%async_computation.5 | async-start | bytes 4718592 | tf_op jit(solution)/shard_map/all_gather | solution.py:131
  8.7 12.7 %copy-start.3 = (bf16[1024,128]{1,0:T(8,128)(2,1)S(1)}, bf16[1024,128]{1,0:T(8,128)(2,1)}, u32[]{:S(2)}) copy-start(bf16[1024,128]{1,0:T(8,128)(2,1)} %param.16) | copy-start | bytes 786436
  8.7 168.8 %reduce-scatter.2.cloned.1.call-start = ((), (), s32[]{:S(2)}) async-start(), calls=%async_computation.3 | async-start | bytes 4718592 | tf_op jit(solution)/shard_map/reduce_scatter | solution.py:85
  8.7 24.8 %collective-permute-start.2 = (bf16[1,2048,128]{2,1,0:T(8,128)(2,1)}, bf16[1,2048,128]{2,1,0:T(8,128)(2,1)S(1)}, u32[]{:S(2)}, u32[]{:S(2)}) collective-permute-start(bf16[1,2048,128]{2,1,0:T(8,128)(2,1)} %param.29), channel_id=1, source_target_pairs={{0,1},{1,2},{2,3},{3,4},{4,5},{5,6},{6,7},{7,0},{8,9},{9,10},{10,1... | collective-permute-start | bytes 1572872 | tf_op jit(solution)/shard_map/ppermute | solution.py:127
  10.7 10.9 %collective-permute-start.1 = (bf16[128,64]{0,1:T(8,128)(2,1)S(1)}, bf16[128,64]{0,1:T(8,128)(2,1)S(1)}, u32[]{:S(2)}, u32[]{:S(2)}) collective-permute-start(bf16[128,64]{0,1:T(8,128)(2,1)S(1)} %slice.36), channel_id=1, source_target_pairs={{0,8},{8,16},{16,24},{1,9},{9,17},{17,25},{2,10},{10,18},{18,26},{... | collective-permute-start | bytes 49160 | tf_op jit(solution)/shard_map/ppermute | solution.py:17
  15.3 7.5 %collective-permute-start = (bf16[128,64]{0,1:T(8,128)(2,1)S(1)}, bf16[128,64]{0,1:T(8,128)(2,1)S(1)}, u32[]{:S(2)}, u32[]{:S(2)}) collective-permute-start(bf16[128,64]{0,1:T(8,128)(2,1)S(1)} %slice.34), channel_id=1, source_target_pairs={{0,8},{8,16},{16,24},{1,9},{9,17},{17,25},{2,10},{10,18},{18,26},{... | collective-permute-start | bytes 49160 | tf_op jit(solution)/shard_map/ppermute | solution.py:17
  26.7 1.3 copy-start.5
  29.8 4.9 %copy-start.10 = (bf16[2048,4]{0,1:T(4,128)(2,1)S(1)}, bf16[2048,4]{0,1:T(4,128)(2,1)}, u32[]{:S(2)}) copy-start(bf16[2048,4]{0,1:T(4,128)(2,1)} %param.26) | copy-start | bytes 49156
  29.8 5.2 %copy-start.11 = (bf16[2048,4]{0,1:T(4,128)(2,1)S(1)}, bf16[2048,4]{0,1:T(4,128)(2,1)}, u32[]{:S(2)}) copy-start(bf16[2048,4]{0,1:T(4,128)(2,1)} %param.27) | copy-start | bytes 49156
  29.8 105.8 %all-to-all-start = ((bf16[4,1,96,2048]{3,2,1,0:T(8,128)(2,1)}), bf16[4,1,96,2048]{3,2,1,0:T(8,128)(2,1)S(1)}, u32[]{:S(2)}, u32[]{:S(2)}) async-start(bf16[4,1,96,2048]{3,2,1,0:T(8,128)(2,1)} %bitcast.20), calls=%async_computation.1 | async-start | bytes 3145728 | tf_op jit(solution)/shard_map/all_to_all | solution.py:119
  33.5 21.8 %collective-permute-start.3 = (bf16[1,2048,128]{2,1,0:T(8,128)(2,1)S(1)}, bf16[1,2048,128]{2,1,0:T(8,128)(2,1)}, u32[]{:S(2)}, u32[]{:S(2)}) collective-permute-start(bf16[1,2048,128]{2,1,0:T(8,128)(2,1)S(1)} %collective-permute-done.2), channel_id=1, source_target_pairs={{0,1},{1,2},{2,3},{3,4},{4,5},{5,6},{6,7},{7,0},{8,9},{9,10},{10,1... | collective-permute-start | bytes 1572872 | tf_op jit(solution)/shard_map/ppermute | solution.py:127
  55.3 14.3 %collective-permute-start.4 = (bf16[1,2048,128]{2,1,0:T(8,128)(2,1)}, bf16[1,2048,128]{2,1,0:T(8,128)(2,1)S(1)}, u32[]{:S(2)}, u32[]{:S(2)}) collective-permute-start(bf16[1,2048,128]{2,1,0:T(8,128)(2,1)} %collective-permute-done.3), channel_id=1, source_target_pairs={{0,1},{1,2},{2,3},{3,4},{4,5},{5,6},{6,7},{7,0},{8,9},{9,10},{10,1... | collective-permute-start | bytes 1572872 | tf_op jit(solution)/shard_map/ppermute | solution.py:127
  69.6 11.7 %collective-permute-start.5 = (bf16[1,2048,128]{2,1,0:T(8,128)(2,1)S(1)}, bf16[1,2048,128]{2,1,0:T(8,128)(2,1)}, u32[]{:S(2)}, u32[]{:S(2)}) collective-permute-start(bf16[1,2048,128]{2,1,0:T(8,128)(2,1)S(1)} %collective-permute-done.4), channel_id=1, source_target_pairs={{0,1},{1,2},{2,3},{3,4},{4,5},{5,6},{6,7},{7,0},{8,9},{9,10},{10,1... | collective-permute-start | bytes 1572872 | tf_op jit(solution)/shard_map/ppermute | solution.py:127
  70.0 2.5 %copy-start.2 = (bf16[1,2048,128]{2,1,0:T(8,128)(2,1)S(1)}, bf16[1,2048,128]{2,1,0:T(8,128)(2,1)}, u32[]{:S(2)}) copy-start(bf16[1,2048,128]{2,1,0:T(8,128)(2,1)} %param.29) | copy-start | bytes 1572868
  81.3 21.2 %collective-permute-start.6 = (bf16[1,2048,128]{2,1,0:T(8,128)(2,1)}, bf16[1,2048,128]{2,1,0:T(8,128)(2,1)S(1)}, u32[]{:S(2)}, u32[]{:S(2)}) collective-permute-start(bf16[1,2048,128]{2,1,0:T(8,128)(2,1)} %collective-permute-done.5), channel_id=1, source_target_pairs={{0,1},{1,2},{2,3},{3,4},{4,5},{5,6},{6,7},{7,0},{8,9},{9,10},{10,1... | collective-permute-start | bytes 1572872 | tf_op jit(solution)/shard_map/ppermute | solution.py:127
  102.5 21.7 %collective-permute-start.7 = (bf16[1,2048,128]{2,1,0:T(8,128)(2,1)S(1)}, bf16[1,2048,128]{2,1,0:T(8,128)(2,1)S(1)}, u32[]{:S(2)}, u32[]{:S(2)}) collective-permute-start(bf16[1,2048,128]{2,1,0:T(8,128)(2,1)S(1)} %collective-permute-done.6), channel_id=1, source_target_pairs={{0,1},{1,2},{2,3},{3,4},{4,5},{5,6},{6,7},{7,0},{8,9},{9,10},{10,1... | collective-permute-start | bytes 1572872 | tf_op jit(solution)/shard_map/ppermute | solution.py:127
  124.3 10.4 %collective-permute-start.8 = (bf16[1,2048,128]{2,1,0:T(8,128)(2,1)S(1)}, bf16[1,2048,128]{2,1,0:T(8,128)(2,1)S(1)}, u32[]{:S(2)}, u32[]{:S(2)}) collective-permute-start(bf16[1,2048,128]{2,1,0:T(8,128)(2,1)S(1)} %collective-permute-done.7), channel_id=1, source_target_pairs={{0,1},{1,2},{2,3},{3,4},{4,5},{5,6},{6,7},{7,0},{8,9},{9,10},{10,1... | collective-permute-start | bytes 1572872 | tf_op jit(solution)/shard_map/ppermute | solution.py:127
  149.6 29.1 %copy-start.6 = (f32[2048]{0:T(1024)S(1)}, f32[2048]{0:T(1024)}, u32[]{:S(2)}) copy-start(f32[2048]{0:T(1024)} %param.22) | copy-start | bytes 24580
  149.6 31.1 %all-to-all-start.1 = ((bf16[4,1,96,2048]{3,2,1,0:T(8,128)(2,1)}), bf16[4,1,96,2048]{3,2,1,0:T(8,128)(2,1)S(1)}, u32[]{:S(2)}, u32[]{:S(2)}) async-start(bf16[4,1,96,2048]{3,2,1,0:T(8,128)(2,1)} %fusion.9), calls=%async_computation.2 | async-start | bytes 3145728 | tf_op jit(solution)/shard_map/all_to_all | solution.py:136
  182.8 4.3 %copy-start.7 = (f32[2048]{0:T(1024)S(1)}, f32[2048]{0:T(1024)}, u32[]{:S(2)}) copy-start(f32[2048]{0:T(1024)} %param.25) | copy-start | bytes 24580
  (2 other events, 1.7 us)
Sparse Core Ops, SparseCore 0:
  9.6 59.0 all-gather.2
  70.3 56.5 all-gather.4
  129.1 48.2 reduce-scatter.1
